TPU v7x, 128 devices: a whole 4x4x4 slice. The times are simulated.
128 devices in a mesh: ep: 16 (over z, x), tp: 8 (over y, core).
Axes of the slice: x: 4, y: 4, z: 4, core: 2. Of those that a mesh axis runs over, the one named last changes fastest.
Arguments:
- tokens: bfloat16 [512, 2048], P('ep'), may hold values from -6 to 6
- norm_gain: float32 [2048], replicated, may hold values from 0.1 to 1.9
- norm_bias: float32 [2048], replicated, may hold values from -3 to 3
- routes: int32 [512, 4], P('ep'), may hold values from 0 to 15, all different within a row; in each aligned block of 32 rows (0 to 31, 32 to 63, ...) at most 16 rows name the same one
- route_weights: float32 [512, 4], P('ep'), may hold values from 0.2 to 1
- gate_w: bfloat16 [16, 2048, 4096], P('ep', None, 'tp'), may hold values from -0.125 to 0.125
- up_w: bfloat16 [16, 2048, 4096], P('ep', None, 'tp'), may hold values from -0.125 to 0.125
- down_w: bfloat16 [16, 4096, 2048], P('ep', 'tp'), may hold values from -0.09375 to 0.09375
Outputs:
- mixed: bfloat16 [512, 2048], P('ep', 'tp')
Inputs may be any that keep to these rules, and one draw needn't show every extreme that they name: `routes`: the 4 experts of a token differ; the rows of one index of ep name no expert more than 16 times, and in every draw some index of ep names some expert exactly 16 times.
All inputs are finite; a program needn't handle non-finite values.
Results may differ from a plain program's by a relative error of at most 0.017.
Values may be sent and summed in bfloat16 or wider, within the bound.
A program may use at most 64 MiB of HBM per device.

v0:
```python
import jax
import jax.numpy as jnp
from jax import lax
from jax.sharding import PartitionSpec as P


def split_up(value, dim, size):
    before, after = (value.shape[:dim], value.shape[dim + 1 :])
    return jnp.moveaxis(value.reshape(*before, size, -1, *after), dim, 0)


def summed_on_arrival(value, axis, dim):
    size = lax.axis_size(axis)
    pieces = lax.all_to_all(split_up(value, dim, size), axis, 0, 0, tiled=True)
    return jnp.sum(pieces.astype(jnp.float32), axis=0)


def layer_norm(tokens, norm_gain, norm_bias):
    values = tokens.astype(jnp.float32)
    centred = values - jnp.mean(values, axis=-1, keepdims=True)
    variance = jnp.mean(centred * centred, axis=-1, keepdims=True)
    return (centred * lax.rsqrt(variance + 1e-05) * norm_gain + norm_bias).astype(jnp.bfloat16)


def body(tokens, norm_gain, norm_bias, routes, route_weights, gate_w, up_w, down_w):
    tok_rows, width = tokens.shape
    topk = routes.shape[1]
    experts = lax.axis_size("ep")
    capacity = 2 * tok_rows * topk // experts
    normed = layer_norm(tokens, norm_gain, norm_bias)
    flat_routes = routes.reshape(-1)
    onehot = (flat_routes[:, None] == jnp.arange(experts, dtype=jnp.int32)[None, :]).astype(
        jnp.int32
    )
    ranks = jnp.sum((jnp.cumsum(onehot, axis=0) - onehot) * onehot, axis=1)
    slots = flat_routes * capacity + ranks
    placed = slots[:, None] == jnp.arange(experts * capacity, dtype=jnp.int32)[None, :]
    picker = jnp.any(placed.reshape(tok_rows, topk, experts * capacity), axis=1).T.astype(
        jnp.bfloat16
    )
    outgoing = jnp.dot(picker, normed, preferred_element_type=jnp.float32).astype(jnp.bfloat16)
    outgoing = outgoing.reshape(experts, capacity, width)
    received = lax.all_to_all(outgoing, "ep", split_axis=0, concat_axis=0, tiled=True)
    sources, items, _ = received.shape
    flat_rows = received.reshape(sources * items, width)
    gate = jnp.dot(flat_rows, gate_w[0], preferred_element_type=jnp.float32)
    up = jnp.dot(flat_rows, up_w[0], preferred_element_type=jnp.float32)
    hidden = (jax.nn.silu(gate) * up).astype(jnp.bfloat16)
    partial_value = jnp.dot(hidden, down_w[0], preferred_element_type=jnp.float32)
    partial_value = partial_value.astype(jnp.bfloat16).astype(jnp.float32)
    summed = summed_on_arrival(partial_value.astype(jnp.bfloat16), "tp", 1).astype(jnp.bfloat16)
    produced = summed.reshape(sources, items, summed.shape[1])
    returned = lax.all_to_all(produced, "ep", split_axis=0, concat_axis=0, tiled=True)
    returned = returned.reshape(experts * capacity, returned.shape[2])
    routed = jnp.dot(placed.astype(jnp.bfloat16), returned, preferred_element_type=jnp.float32)
    routed = routed.reshape(tok_rows, topk, routed.shape[1])
    result = jnp.sum(route_weights[:, :, None] * routed, axis=1)
    return result.astype(jnp.bfloat16)


def solution(mesh):
    placed = (
        P("ep", None),
        P(),
        P(),
        P("ep", None),
        P("ep", None),
        P("ep", None, "tp"),
        P("ep", None, "tp"),
        P("ep", "tp", None),
    )
    return jax.shard_map(body, mesh=mesh, in_specs=placed, out_specs=P("ep", "tp"), check_vma=False)
```

profile of v0, /device:TPU:0, one launch (start us, length us, event | category | flops | bytes accessed | tf_op | source)
XLA Modules:
  0.0 70.2 jit_solution(6326663567810828502)
XLA Ops:
  0.0 0.0 copy-start
  0.0 1.2 %convert_reduce_fusion = f32[32]{0:T(128)S(1)} fusion(bf16[32,2048]{1,0:T(8,128)(2,1)} %param.8), kind=kLoop, calls=%fused_computation.18 | loop fusion | flops 131040 | bytes 131200 | tf_op jit(solution)/shard_map/reduce_sum | solution.py:20
  1.2 1.1 %fusion.21 = f32[32]{0:T(128)S(1)} fusion(bf16[32,2048]{1,0:T(8,128)(2,1)} %param.8, f32[32]{0:T(128)S(1)} %broadcast_multiply_fusion), kind=kLoop, calls=%fused_computation.21 | loop fusion | flops 262112 | bytes 131328 | tf_op jit(solution)/shard_map/reduce_sum | solution.py:21
  2.3 0.8 %copy.28 = s32[32,4]{1,0:T(8,128)S(1)} copy(s32[32,4]{0,1:T(4,128)} %param.11) | data formatting | bytes 1024 | tf_op args[3]
  3.1 0.1 eq.51
  3.2 0.1 fusion.35
  3.3 0.2 reduce_window_sum.11
  3.5 0.2 select_reduce_fusion
  3.6 0.1 reduce_sum.51
  3.8 0.1 copy.29
  3.8 0.0 copy-start.1
  3.8 0.8 %multiply_add_fusion = s32[32,4]{0,1:T(4,128)S(1)} fusion(s32[32,4]{0,1:T(4,128)S(1)} %copy.29, s32[32,4]{0,1:T(4,128)} %param.11), kind=kLoop, calls=%fused_computation.38 | loop fusion | flops 256 | bytes 1536 | tf_op jit(solution)/shard_map/add | solution.py:36
  4.7 0.1 fusion.33
  4.8 1.4 %convolution_convert_fusion.1 = bf16[256,2048]{1,0:T(8,128)(2,1)S(1)} fusion(pred[32,256]{1,0:T(8,128)(4,1)S(1)} %fusion.33, bf16[32,2048]{1,0:T(8,128)(2,1)} %param.8, f32[2048]{0:T(1024)} %param.10, f32[2048]{0:T(1024)} %param.9, f32[32]{0:T(128)S(1)} %add_rsqrt_fusion, f32[32]{0:T(128)S(1)} %broadcast_multiply_fusion), kind=kOutput, calls=%fused_computation.1 | convolution fusion | flops 34471936 | bytes 1204480 | tf_op jit(solution)/shard_map/dot_general | solution.py:41
  6.2 24.9 %all_to_all.15 = bf16[16,16,2048]{2,1,0:T(8,128)(2,1)S(1)} all-to-all(bf16[16,16,2048]{2,1,0:T(8,128)(2,1)S(1)} %bitcast.35), channel_id=1, replica_groups=mesh['ep'=16,'tp'=8] {'ep'}, dimensions={0} | all-to-all | bytes 2097152 | tf_op jit(solution)/shard_map/all_to_all | solution.py:43
  31.2 0.0 copy-done.1
  31.2 1.6 %fusion.3 = f32[256,512]{1,0:T(8,128)} fusion(bf16[256,2048]{1,0:T(8,128)(2,1)S(1)} %bitcast.37, bf16[1,2048,512]{2,1,0:T(8,128)(2,1)S(1)} %copy-done.1), kind=kOutput, calls=%fused_computation.5 | convolution fusion | flops 536870912 | bytes 3670016 | tf_op jit(solution)/shard_map/dot_general | solution.py:46
  32.7 0.0 copy-done
  32.7 4.0 %convolution_convert_fusion = bf16[256,2048]{1,0:T(8,128)(2,1)} fusion(bf16[1,512,2048]{2,1,0:T(8,128)(2,1)S(1)} %copy-done, bf16[256,2048]{1,0:T(8,128)(2,1)S(1)} %bitcast.38, bf16[1,2048,512]{2,1,0:T(8,128)(2,1)} %param.14, f32[256,512]{1,0:T(8,128)} %fusion.3), kind=kOutput, calls=%fused_computation | convolution fusion | flops 1075052544 | bytes 6815744 | tf_op jit(solution)/shard_map/dot_general | solution.py:49
  36.8 1.3 %copy.33 = bf16[32,8,8,256]{3,2,0,1:T(8,128)(2,1)S(1)} copy(bf16[32,8,8,256]{3,2,1,0:T(8,128)(2,1)} %bitcast.39) | data formatting | bytes 2097152 | tf_op jit(solution)/shard_map/reshape | solution.py:9
  38.0 0.0 copy-start.2
  38.1 20.2 %all_to_all.16 = bf16[8,256,256]{2,1,0:T(8,128)(2,1)S(1)} all-to-all(bf16[8,256,256]{2,1,0:T(8,128)(2,1)S(1)} %bitcast.36), channel_id=1, replica_groups=mesh['ep'=16,'tp'=8] {'tp'}, dimensions={0} | all-to-all | bytes 2097152 | tf_op jit(solution)/shard_map/all_to_all | solution.py:14
  58.3 0.1 reduce_sum.54
  58.5 10.9 %all_to_all.17 = bf16[16,16,256]{2,1,0:T(8,128)(2,1)S(1)} all-to-all(bf16[16,16,256]{2,1,0:T(8,128)(2,1)S(1)} %bitcast.40), channel_id=1, replica_groups=mesh['ep'=16,'tp'=8] {'ep'}, dimensions={0} | all-to-all | bytes 262144 | tf_op jit(solution)/shard_map/all_to_all | solution.py:53
  69.4 0.0 copy-done.2
  69.4 0.8 %fusion.11 = bf16[32,256]{1,0:T(8,128)(2,1)} fusion(bf16[256,256,1]{1,0,2:T(8,128)(2,1)S(1)} %bitcast.41, s32[32,4]{0,1:T(4,128)S(1)} %multiply_add_fusion, f32[32,4]{0,1:T(4,128)S(1)} %copy-done.2), kind=kOutput, calls=%fused_computation.10 | convolution fusion | flops 16867328 | bytes 148480 | tf_op jit(solution)/shard_map/dot_general | solution.py:55
  (2 shorter events, 0.0 us)
Async XLA Ops:
  0.0 32.7 %copy-start = (bf16[1,512,2048]{2,1,0:T(8,128)(2,1)S(1)}, bf16[1,512,2048]{2,1,0:T(8,128)(2,1)}, u32[]{:S(2)}) copy-start(bf16[1,512,2048]{2,1,0:T(8,128)(2,1)} %param.15) | copy-start | bytes 6291460
  3.8 27.3 %copy-start.1 = (bf16[1,2048,512]{2,1,0:T(8,128)(2,1)S(1)}, bf16[1,2048,512]{2,1,0:T(8,128)(2,1)}, u32[]{:S(2)}) copy-start(bf16[1,2048,512]{2,1,0:T(8,128)(2,1)} %param.13) | copy-start | bytes 6291460
  38.0 31.4 %copy-start.2 = (f32[32,4]{0,1:T(4,128)S(1)}, f32[32,4]{0,1:T(4,128)}, u32[]{:S(2)}) copy-start(f32[32,4]{0,1:T(4,128)} %param.12) | copy-start | bytes 1540
where the time goes:
time: 70.6 us; the launch traced here: 70.2 us
  blocking collectives  56.1 us (79%)
  matrix products  7.84 us (11%)
  other arithmetic  3.82 us (5%)
  local copies, waits for them, and re-layouts  2.36 us (3%)
    all_to_all x1, blocking collectives, body(): lax.all_to_all(outgoing, 'ep', split_axis=0, concat_axis=0, tiled=True)  24.9 us
    all_to_all x1, blocking collectives, summed_on_arrival(): pieces = lax.all_to_all(split_up(value, dim, size), axis, 0, 0, tiled=True)  20.2 us
    all_to_all x1, blocking collectives, body(): lax.all_to_all(produced, 'ep', split_axis=0, concat_axis=0, tiled=True)  10.9 us
    dot_general x1, matrix products, body(): jnp.dot(hidden, down_w[0], preferred_element_type=jnp.float32)  4.04 us
    dot_general x1, matrix products, body(): gate = jnp.dot(flat_rows, gate_w[0], preferred_element_type=jnp.float32)  1.56 us
    dot_general x1, matrix products, body(): jnp.dot(picker, normed, preferred_element_type=jnp.float32)  1.43 us

commit v1 on v0

v1 whole, which is shorter than its diff:
```python
import functools

import jax
import jax.numpy as jnp
from jax import lax
from jax.experimental import pallas as pl
from jax.experimental.pallas import tpu as pltpu
from jax.sharding import PartitionSpec as P

MESH = pl.DeviceIdType.MESH
SIDE = 4
CAP = 16
N_Y = 4
BLK = 256


def offset(k, j):
    dz = j // 2
    return dz, 2 * (j % 2) + (k + dz) % 2


def kernel(
    tok_hbm, gain_hbm, bias_hbm, routes_hbm, weights_hbm, gate_hbm, up_hbm, down_hbm,
    out_ref,
    tok, gain, bias, routes, weights, w_in, w_out, swap_in, swap_out,
    out_buf, x_buf, y_buf, r_buf, z_buf, z_own, zr_buf,
    load_sem, wload_sem, swap_send, swap_recv, d_send, d_recv, r_send, r_recv, z_send, z_recv,
):
    ep, tp = lax.axis_index("ep"), lax.axis_index("tp")
    z, x = ep // SIDE, ep % SIDE
    y, c = tp // 2, tp % 2
    k = (z + x + c) % 2
    par = (z + x) % 2

    small = [
        pltpu.make_async_copy(src, dst, load_sem.at[i])
        for i, (src, dst) in enumerate(
            ((tok_hbm, tok), (gain_hbm, gain), (bias_hbm, bias), (routes_hbm, routes), (weights_hbm, weights))
        )
    ]
    for copy in small:
        copy.start()
    big = [
        pltpu.make_async_copy(gate_hbm.at[0], w_in.at[0], wload_sem.at[0]),
        pltpu.make_async_copy(up_hbm.at[0], w_in.at[1], wload_sem.at[1]),
        pltpu.make_async_copy(down_hbm.at[0], w_out, wload_sem.at[2]),
    ]
    for copy in big:
        copy.start()

    barrier = pltpu.get_barrier_semaphore()
    for dz in range(SIDE):
        for dx in range(SIDE):
            for dc in range(2):
                if dz or dx or dc:
                    pl.semaphore_signal(
                        barrier, inc=1,
                        device_id=(((z + dz) % SIDE) * SIDE + (x + dx) % SIDE, y * 2 + (c + dc) % 2),
                        device_id_type=MESH,
                    )
    for dy in range(1, N_Y):
        pl.semaphore_signal(barrier, inc=1, device_id=(ep, ((y + dy) % N_Y) * 2 + c), device_id_type=MESH)

    for copy in small:
        copy.wait()
    rows = tok.shape[0]
    values = tok[...].astype(jnp.float32)
    centred = values - jnp.mean(values, axis=-1, keepdims=True)
    variance = jnp.mean(centred * centred, axis=-1, keepdims=True)
    normed = (centred * lax.rsqrt(variance + 1e-05) * gain[...] + bias[...]).astype(jnp.bfloat16)

    width = 2 * 8 * CAP
    col = lax.broadcasted_iota(jnp.int32, (rows, width), 1)
    dz = (col // (2 * CAP)) % 4
    dx = 2 * ((col // CAP) % 2) + (col // (8 * CAP) + dz) % 2
    expert = ((z + dz) % SIDE) * SIDE + (x + dx) % SIDE
    named = jnp.zeros((rows, width), jnp.float32)
    weight = jnp.zeros((rows, width), jnp.float32)
    for i in range(routes.shape[1]):
        hit = routes[:, i : i + 1] == expert
        named = jnp.where(hit, 1.0, named)
        weight = jnp.where(hit, weights[:, i : i + 1], weight)
    earlier = (
        lax.broadcasted_iota(jnp.int32, (rows, rows), 1) < lax.broadcasted_iota(jnp.int32, (rows, rows), 0)
    ).astype(jnp.float32).astype(jnp.bfloat16)
    rank = jnp.dot(earlier, named.astype(jnp.bfloat16), preferred_element_type=jnp.float32)
    here = (named > 0.5) & (rank == (col % CAP).astype(jnp.float32))
    picker = jnp.where(here, 1.0, 0.0)
    mine = jnp.where(k == 0, picker[:, : width // 2], picker[:, width // 2 :]).astype(jnp.bfloat16)
    outgoing = lax.dot_general(mine, normed, (((0,), (0,)), ((), ())), preferred_element_type=jnp.float32)
    out_buf[...] = outgoing.astype(jnp.bfloat16).reshape(out_buf.shape)

    pl.semaphore_wait(barrier, 2 * SIDE * SIDE - 1 + N_Y - 1)

    sibling = (ep, y * 2 + 1 - c)
    swaps = []
    for i, (src, dst) in enumerate(((w_in.at[0], swap_in.at[0]), (w_in.at[1], swap_in.at[1]), (w_out, swap_out))):
        swaps.append(
            pltpu.make_async_remote_copy(
                src_ref=src, dst_ref=dst, send_sem=swap_send.at[i], recv_sem=swap_recv.at[i],
                device_id=sibling, device_id_type=MESH,
            )
        )

    def dispatch(j):
        dz, dx = offset(k, j)
        return pltpu.make_async_remote_copy(
            src_ref=out_buf.at[j], dst_ref=x_buf.at[j], send_sem=d_send.at[j], recv_sem=d_recv.at[j],
            device_id=(((z + dz) % SIDE) * SIDE + (x + dx) % SIDE, y * 2 + par), device_id_type=MESH,
        )

    order = (5, 4, 1, 2, 3, 6, 7)
    for j in order:
        dispatch(j).start()

    @pl.when(k == 1)
    def _():
        dispatch(0).start()

    @pl.when(k == 0)
    def _():
        x_buf[0] = out_buf[0]

    for load, swap in zip(big, swaps):
        load.wait()
        swap.start()

    for j in order:
        dispatch(j).wait_recv()

    @pl.when(k == 1)
    def _():
        dispatch(0).wait_recv()

    def hidden_of(both):
        rows_in = x_buf[...].reshape(8 * CAP, x_buf.shape[2])
        gate = jnp.dot(rows_in, both[0], preferred_element_type=jnp.float32)
        up = jnp.dot(rows_in, both[1], preferred_element_type=jnp.float32)
        return (gate / (1.0 + jnp.exp(-gate)) * up).astype(jnp.bfloat16)

    hidden_own = hidden_of(w_in)
    swaps[0].wait_recv()
    swaps[1].wait_recv()
    hidden_swap = hidden_of(swap_in)
    swaps[2].wait_recv()

    def give_back(h, j):
        dz, dx = offset(k, j)
        return pltpu.make_async_remote_copy(
            src_ref=y_buf.at[h, j], dst_ref=r_buf.at[k * 8 + j], send_sem=r_send.at[h, j], recv_sem=r_recv.at[k * 8 + j],
            device_id=(((z - dz + SIDE) % SIDE) * SIDE + (x - dx + SIDE) % SIDE, y * 2 + h), device_id_type=MESH,
        )

    for h in range(2):
        for part in range(N_Y):
            cols = pl.ds((2 * part + h) * BLK, BLK)
            piece = jnp.dot(hidden_own, w_out[:, cols], preferred_element_type=jnp.float32)
            piece += jnp.dot(hidden_swap, swap_out[:, cols], preferred_element_type=jnp.float32)
            y_buf[h, :, :, part * BLK : (part + 1) * BLK] = piece.astype(jnp.bfloat16).reshape(8, CAP, BLK)
        for j in order:
            give_back(h, j).start()
        local = (k == 0) & (c == h)

        @pl.when(local)
        def _():
            r_buf[0] = y_buf[h, 0]

        @pl.when(jnp.logical_not(local))
        def _():
            give_back(h, 0).start()

    def arrival(i):
        return pltpu.make_async_remote_copy(
            src_ref=y_buf.at[0, 0], dst_ref=r_buf.at[i], send_sem=r_send.at[0, 0], recv_sem=r_recv.at[i],
            device_id=sibling, device_id_type=MESH,
        )

    for i in range(1, 16):
        arrival(i).wait_recv()

    @pl.when(k == 1)
    def _():
        arrival(0).wait_recv()

    scaled = jnp.where(here, weight, 0.0)
    high = scaled.astype(jnp.bfloat16)
    low = (scaled - high.astype(jnp.float32)).astype(jnp.bfloat16)
    both = jnp.concatenate([high, low], axis=0)
    for part in range(N_Y):
        got = r_buf[:, :, part * BLK : (part + 1) * BLK].reshape(16 * CAP, BLK)
        twice = jnp.dot(both, got, preferred_element_type=jnp.float32)
        summed = twice[:rows] + twice[rows:]
        z_own[part] = summed
        z_buf[part] = summed.astype(jnp.bfloat16)

    def across(i):
        there = (y + i) % N_Y
        return pltpu.make_async_remote_copy(
            src_ref=z_buf.at[there], dst_ref=zr_buf.at[i - 1], send_sem=z_send.at[i - 1], recv_sem=z_recv.at[i - 1],
            device_id=(ep, there * 2 + c), device_id_type=MESH,
        )

    for i in (2, 1, 3):
        across(i).start()
    total = z_own[y]
    for i in (1, 3, 2):
        across(i).wait_recv()
    for i in range(3):
        total += zr_buf[i].astype(jnp.float32)
    out_ref[...] = total.astype(out_ref.dtype)

    for swap in swaps:
        swap.wait_send()
    for j in order:
        dispatch(j).wait_send()

    @pl.when(k == 1)
    def _():
        dispatch(0).wait_send()

    for h in range(2):
        for j in order:
            give_back(h, j).wait_send()

        @pl.when(jnp.logical_not((k == 0) & (c == h)))
        def _():
            give_back(h, 0).wait_send()
    for i in range(1, N_Y):
        across(i).wait_send()


def body(tokens, norm_gain, norm_bias, routes, route_weights, gate_w, up_w, down_w):
    rows, width = tokens.shape
    half = gate_w.shape[2]
    any_ = pl.BlockSpec(memory_space=pl.ANY)
    bf16, f32 = jnp.bfloat16, jnp.float32
    dma = pltpu.SemaphoreType.DMA
    return pl.pallas_call(
        kernel,
        name="moe",
        out_shape=jax.ShapeDtypeStruct((rows, BLK), bf16),
        in_specs=[any_] * 8,
        out_specs=pl.BlockSpec(memory_space=pltpu.VMEM),
        scratch_shapes=[
            pltpu.VMEM((rows, width), bf16),
            pltpu.VMEM((1, width), f32),
            pltpu.VMEM((1, width), f32),
            pltpu.VMEM(routes.shape, jnp.int32),
            pltpu.VMEM(route_weights.shape, f32),
            pltpu.VMEM((2, width, half), bf16),
            pltpu.VMEM((half, width), bf16),
            pltpu.VMEM((2, width, half), bf16),
            pltpu.VMEM((half, width), bf16),
            pltpu.VMEM((8, CAP, width), bf16),
            pltpu.VMEM((8, CAP, width), bf16),
            pltpu.VMEM((2, 8, CAP, width // 2), bf16),
            pltpu.VMEM((16, CAP, width // 2), bf16),
            pltpu.VMEM((N_Y, rows, BLK), bf16),
            pltpu.VMEM((N_Y, rows, BLK), f32),
            pltpu.VMEM((N_Y - 1, rows, BLK), bf16),
            dma((5,)), dma((3,)), dma((3,)), dma((3,)), dma((8,)), dma((8,)), dma((2, 8)), dma((16,)), dma((3,)), dma((3,)),
        ],
        compiler_params=pltpu.CompilerParams(collective_id=0, has_side_effects=True),
    )(
        tokens, norm_gain.reshape(1, width), norm_bias.reshape(1, width), routes, route_weights, gate_w, up_w, down_w
    )


def solution(mesh):
    placed = (
        P("ep", None),
        P(),
        P(),
        P("ep", None),
        P("ep", None),
        P("ep", None, "tp"),
        P("ep", None, "tp"),
        P("ep", "tp", None),
    )
    return jax.shard_map(body, mesh=mesh, in_specs=placed, out_specs=P("ep", "tp"), check_vma=False)
```

time: 70.6 us -> 37.1 us (0.53)
  the two profiles are of different devices: /device:TPU:0 before, /device:TPU:1 now
where the time goes in v1:
time: 37.1 us; the launch traced here: 36.9 us
  Pallas kernels  32.8 us (88%)
  local copies, waits for them, and re-layouts  4.05 us (11%)
    pallas_call x1, Pallas kernels, body(): pl.pallas_call(kernel, name='moe', out_shape=jax.ShapeDtypeStruct((rows,...  32.8 us
    unnamed x3, local copies, waits for them, and re-layouts  4.05 us

profile of v1, /device:TPU:1, one launch (start us, length us, event | category | flops | bytes accessed | tf_op | source)
XLA Modules:
  0.0 36.9 jit_solution(8142554133656007694)
XLA Ops:
  0.0 1.4 %copy.9.routes_hbm = s32[32,4]{1,0:T(8,128)} copy(s32[32,4]{0,1:T(4,128)} %param.11) | data formatting | bytes 1024 | tf_op args[3]
  1.4 1.4 %copy.10.weights_hbm = f32[32,4]{1,0:T(8,128)} copy(f32[32,4]{0,1:T(4,128)} %param.12) | data formatting | bytes 1024 | tf_op args[4]
  2.7 32.8 %moe.1 = bf16[32,256]{1,0:T(8,128)(2,1)} custom-call(bf16[32,2048]{1,0:T(8,128)(2,1)} %tok_hbm.1, f32[1,2048]{1,0:T(1,128)} %bitcast.2, f32[1,2048]{1,0:T(1,128)} %bitcast.3, s32[32,4]{1,0:T(8,128)} %copy.9.routes_hbm, f32[32,4]{1,0:T(8,128)} %copy.10.weights_hbm, bf16[1,2048,512]{2,1,0:T(8,128)(2,1)} %gate_hbm.1, bf16[1,2048,512]{2,1,0:T(8,128)(2,1)} %up_hbm.1, ...), custom_call_target="tpu_custom_call" | custom-call | tf_op jit(solution)/shard_map/moe/pallas_call | solution.py:238
  35.5 1.3 %copy.12 = bf16[32,256]{1,0:T(8,128)(2,1)} copy(bf16[32,256]{1,0:T(8,128)(2,1)} %moe.1) | data formatting | bytes 32768

commit v2 on v1

v2 whole, which is shorter than its diff:
```python
import jax
import jax.numpy as jnp
from jax import lax
from jax.experimental import pallas as pl
from jax.experimental.pallas import tpu as pltpu
from jax.sharding import PartitionSpec as P

MESH = pl.DeviceIdType.MESH
SIDE = 4
CAP = 16
BLK = 256
CHUNKS = 1
OFFSETS = (
    ((2, 2), (1, 1), (3, 3), (1, 3), (3, 1), (0, 2), (2, 0), (0, 0)),
    ((1, 2), (2, 1), (3, 2), (2, 3), (0, 1), (0, 3), (1, 0), (3, 0)),
)


def offset(k, i):
    (z0, x0), (z1, x1) = OFFSETS[0][i], OFFSETS[1][i]
    return z0 + k * (z1 - z0), x0 + k * (x1 - x0)


def packed(which):
    word = 0
    for n, pair in enumerate(OFFSETS[1] + OFFSETS[0]):
        word |= pair[which] << (2 * n)
    return word - (1 << 32) if word >= 1 << 31 else word


def kernel(
    tok_hbm, gain_hbm, bias_hbm, routes_hbm, weights_hbm, gate_hbm, up_hbm, down_hbm,
    out_ref,
    tok, gain, bias, routes, weights, w_in, w_out, swap_in, swap_out,
    out_buf, x_buf, y_buf, r_buf,
    load_sem, wload_sem, swap_send, swap_recv, d_send, d_recv, r_send, r_recv, plane_sem,
):
    ep, tp = lax.axis_index("ep"), lax.axis_index("tp")
    z, x = ep // SIDE, ep % SIDE
    y, c = tp // 2, tp % 2
    par = (z + x) % 2
    k = (par + c) % 2

    def chip(dz, dx):
        return ((z + dz) % SIDE) * SIDE + (x + dx) % SIDE

    small = [
        pltpu.make_async_copy(src, dst, load_sem.at[i])
        for i, (src, dst) in enumerate(
            ((tok_hbm, tok), (gain_hbm, gain), (bias_hbm, bias), (routes_hbm, routes), (weights_hbm, weights))
        )
    ]
    for copy in small:
        copy.start()
    big = [
        pltpu.make_async_copy(gate_hbm.at[0], w_in.at[0], wload_sem.at[0]),
        pltpu.make_async_copy(up_hbm.at[0], w_in.at[1], wload_sem.at[1]),
        pltpu.make_async_copy(down_hbm.at[0], w_out, wload_sem.at[2]),
    ]
    for copy in big:
        copy.start()

    barrier = pltpu.get_barrier_semaphore()
    for dz in range(SIDE):
        for dx in range(SIDE):
            for dc in range(2):
                if dz or dx or dc:
                    pl.semaphore_signal(
                        barrier, inc=1, device_id=(chip(dz, dx), y * 2 + (c + dc) % 2), device_id_type=MESH
                    )
    column = [(ep, ((y + dy) % SIDE) * 2 + c) for dy in range(1, SIDE)]
    for there in column:
        pl.semaphore_signal(barrier, inc=1, device_id=there, device_id_type=MESH)

    for copy in small:
        copy.wait()
    rows = tok.shape[0]
    values = tok[...].astype(jnp.float32)
    centred = values - jnp.mean(values, axis=-1, keepdims=True)
    variance = jnp.mean(centred * centred, axis=-1, keepdims=True)
    normed = (centred * lax.rsqrt(variance + 1e-05) * gain[...] + bias[...]).astype(jnp.bfloat16)

    slots = 16 * CAP
    slot = lax.broadcasted_iota(jnp.int32, (slots, rows), 0)
    shift = 2 * (slot // CAP)
    dz = lax.shift_right_logical(jnp.full_like(slot, packed(0)), shift) & 3
    dx = lax.shift_right_logical(jnp.full_like(slot, packed(1)), shift) & 3
    expert = ((z + dz) & 3) * SIDE + ((x + dx) & 3)
    named = jnp.zeros((slots, rows), jnp.float32)
    weight = jnp.zeros((slots, rows), jnp.float32)
    for i in range(routes.shape[0]):
        hit = routes[i : i + 1, :] == expert
        named = jnp.where(hit, 1.0, named)
        weight = jnp.where(hit, weights[i : i + 1, :], weight)
    earlier = (
        lax.broadcasted_iota(jnp.int32, (rows, rows), 0) < lax.broadcasted_iota(jnp.int32, (rows, rows), 1)
    ).astype(jnp.float32).astype(jnp.bfloat16)
    rank = jnp.dot(named.astype(jnp.bfloat16), earlier, preferred_element_type=jnp.float32)
    here = (named > 0.5) & (rank == (slot % CAP).astype(jnp.float32))
    picker = jnp.where(here, 1.0, 0.0)
    mine = jnp.where(k == 1, picker[: slots // 2], picker[slots // 2 :]).astype(jnp.bfloat16)
    outgoing = jnp.dot(mine, normed, preferred_element_type=jnp.float32)
    out_buf[...] = outgoing.astype(jnp.bfloat16).reshape(out_buf.shape)

    pl.semaphore_wait(barrier, 2 * SIDE * SIDE - 1 + SIDE - 1)

    sibling = (ep, y * 2 + 1 - c)
    swaps = []
    for i, (src, dst) in enumerate(((w_in.at[0], swap_in.at[0]), (w_in.at[1], swap_in.at[1]), (w_out, swap_out))):
        swaps.append(
            pltpu.make_async_remote_copy(
                src_ref=src, dst_ref=dst, send_sem=swap_send.at[i], recv_sem=swap_recv.at[i],
                device_id=sibling, device_id_type=MESH,
            )
        )

    def dispatch(i):
        dz, dx = offset(k, i)
        return pltpu.make_async_remote_copy(
            src_ref=out_buf.at[i], dst_ref=x_buf.at[i], send_sem=d_send.at[i], recv_sem=d_recv.at[i],
            device_id=(chip(dz, dx), y * 2 + par), device_id_type=MESH,
        )

    for i in range(7):
        dispatch(i).start()

    @pl.when(k == 1)
    def _():
        dispatch(7).start()

    @pl.when(k == 0)
    def _():
        x_buf[7] = out_buf[7]

    for there in column:
        pl.semaphore_signal(plane_sem, inc=1, device_id=there, device_id_type=MESH)

    for load, swap in zip(big, swaps):
        load.wait()
        swap.start()

    def hidden_of(rows_in, both):
        gate = jnp.dot(rows_in, both[0], preferred_element_type=jnp.float32)
        up = jnp.dot(rows_in, both[1], preferred_element_type=jnp.float32)
        return (gate / (1.0 + jnp.exp(-gate)) * up).astype(jnp.bfloat16)

    def give_back(i, dy, h):
        dz, dx = offset(k, i)
        own = i == 7 and dy == 0
        return pltpu.make_async_remote_copy(
            src_ref=y_buf.at[i, dy, h], dst_ref=r_buf.at[dy, (1 - k) * 8 + i],
            send_sem=r_send.at[h + 1 if own else 0 if i < 7 else 3],
            recv_sem=r_recv.at[4 * (1 - k) if own else dy],
            device_id=(chip(SIDE - dz, SIDE - dx), ((y + dy) % SIDE) * 2 + h), device_id_type=MESH,
        )

    per = 8 // CHUNKS
    for chunk in range(CHUNKS):
        first = chunk * per
        for i in range(first, first + per):
            if i < 7:
                dispatch(i).wait_recv()
            else:

                @pl.when(k == 1)
                def _():
                    dispatch(7).wait_recv()

        rows_in = x_buf[first : first + per].reshape(per * CAP, x_buf.shape[2])
        hidden_own = hidden_of(rows_in, w_in)
        if chunk == 0:
            swaps[0].wait_recv()
            swaps[1].wait_recv()
        hidden_swap = hidden_of(rows_in, swap_in)
        if chunk == 0:
            swaps[2].wait_recv()
            pl.semaphore_wait(plane_sem, SIDE - 1)
        for dy in (2, 1, 3, 0):
            for h in range(2):
                cols = pl.ds(pl.multiple_of((((y + dy) % SIDE) * 2 + h) * BLK, BLK), BLK)
                piece = jnp.dot(hidden_own, w_out[:, cols], preferred_element_type=jnp.float32)
                piece += jnp.dot(hidden_swap, swap_out[:, cols], preferred_element_type=jnp.float32)
                y_buf[first : first + per, dy, h] = piece.astype(jnp.bfloat16).reshape(per, CAP, BLK)
            for i in range(first, first + per):
                for h in range(2):
                    if i < 7 or dy:
                        give_back(i, dy, h).start()
                    else:
                        local = (k == 0) & (c == h)

                        @pl.when(local)
                        def _():
                            r_buf[0, 15] = y_buf[7, 0, h]

                        @pl.when(jnp.logical_not(local))
                        def _():
                            give_back(7, 0, h).start()

    scaled = jnp.where(here, weight, 0.0).T
    high = scaled.astype(jnp.bfloat16)
    low = (scaled - high.astype(jnp.float32)).astype(jnp.bfloat16)
    both = jnp.concatenate([high, low], axis=0)

    def arrived(blocks, sem):
        return pltpu.make_async_remote_copy(
            src_ref=blocks, dst_ref=blocks, send_sem=r_send.at[0], recv_sem=r_recv.at[sem],
            device_id=sibling, device_id_type=MESH,
        )

    arrived(r_buf.at[0, 0:15], 0).wait_recv()

    @pl.when(k == 1)
    def _():
        arrived(r_buf.at[0, 15], 4).wait_recv()

    for dy in (1, 3, 2):
        arrived(r_buf.at[dy], dy).wait_recv()
    twice = jnp.zeros((2 * rows, BLK), jnp.float32)
    for dy in range(SIDE):
        twice += jnp.dot(both, r_buf[dy].reshape(slots, BLK), preferred_element_type=jnp.float32)
    out_ref[...] = (twice[:rows] + twice[rows:]).astype(out_ref.dtype)

    for swap in swaps:
        swap.wait_send()
    for i in range(7):
        dispatch(i).wait_send()

    @pl.when(k == 1)
    def _():
        dispatch(7).wait_send()

    def sent(blocks, sem):
        return pltpu.make_async_remote_copy(
            src_ref=blocks, dst_ref=blocks, send_sem=r_send.at[sem], recv_sem=r_recv.at[0],
            device_id=sibling, device_id_type=MESH,
        )

    sent(y_buf.at[0:7], 0).wait_send()
    sent(y_buf.at[7, 1:4], 3).wait_send()
    for h in range(2):

        @pl.when(jnp.logical_not((k == 0) & (c == h)))
        def _():
            sent(y_buf.at[7, 0, h], h + 1).wait_send()


def body(tokens, norm_gain, norm_bias, routes, route_weights, gate_w, up_w, down_w):
    rows, width = tokens.shape
    half = gate_w.shape[2]
    hbm = pl.BlockSpec(memory_space=pl.ANY)
    bf16, f32 = jnp.bfloat16, jnp.float32
    dma = pltpu.SemaphoreType.DMA
    return pl.pallas_call(
        kernel,
        name="moe",
        out_shape=jax.ShapeDtypeStruct((rows, BLK), bf16),
        in_specs=[hbm] * 8,
        out_specs=pl.BlockSpec(memory_space=pltpu.VMEM),
        scratch_shapes=[
            pltpu.VMEM((rows, width), bf16),
            pltpu.VMEM((1, width), f32),
            pltpu.VMEM((1, width), f32),
            pltpu.VMEM(routes.shape[::-1], jnp.int32),
            pltpu.VMEM(route_weights.shape[::-1], f32),
            pltpu.VMEM((2, width, half), bf16),
            pltpu.VMEM((half, width), bf16),
            pltpu.VMEM((2, width, half), bf16),
            pltpu.VMEM((half, width), bf16),
            pltpu.VMEM((8, CAP, width), bf16),
            pltpu.VMEM((8, CAP, width), bf16),
            pltpu.VMEM((8, SIDE, 2, CAP, BLK), bf16),
            pltpu.VMEM((SIDE, 16, CAP, BLK), bf16),
            dma((5,)), dma((3,)), dma((3,)), dma((3,)), dma((8,)), dma((8,)), dma((4,)), dma((5,)),
            pltpu.SemaphoreType.REGULAR,
        ],
        compiler_params=pltpu.CompilerParams(collective_id=0, has_side_effects=True),
    )(
        tokens, norm_gain.reshape(1, width), norm_bias.reshape(1, width), routes.T, route_weights.T, gate_w, up_w, down_w
    )


def solution(mesh):
    placed = (
        P("ep", None),
        P(),
        P(),
        P("ep", None),
        P("ep", None),
        P("ep", None, "tp"),
        P("ep", None, "tp"),
        P("ep", "tp", None),
    )
    return jax.shard_map(body, mesh=mesh, in_specs=placed, out_specs=P("ep", "tp"), check_vma=False)
```

time: 37.1 us -> 32.4 us (0.87)
  local copies, waits for them, and re-layouts: 4.05 us -> 1.32 us
  Pallas kernels: 32.8 us -> 30.8 us
    unnamed x3 -> x1, local copies, waits for them, and re-layouts: 4.05 us -> 1.32 us
    pallas_call x1, Pallas kernels: 32.8 us -> 30.8 us  [body(): pl.pallas_call(kernel, name='moe', out_shape=jax.ShapeDtypeStruct((rows,...]
where the time goes in v2:
time: 32.4 us; the launch traced here: 32.2 us
  Pallas kernels  30.8 us (95%)
  local copies, waits for them, and re-layouts  1.32 us (4%)
    pallas_call x1, Pallas kernels, body(): pl.pallas_call(kernel, name='moe', out_shape=jax.ShapeDtypeStruct((rows,...  30.8 us
    unnamed x1, local copies, waits for them, and re-layouts  1.32 us

profile of v2, /device:TPU:1, one launch (start us, length us, event | category | flops | bytes accessed | tf_op | source)
XLA Modules:
  0.0 32.2 jit_solution(15530225130234772807)
XLA Ops:
  0.0 30.8 %moe.1 = bf16[32,256]{1,0:T(8,128)(2,1)} custom-call(bf16[32,2048]{1,0:T(8,128)(2,1)} %tok_hbm.1, f32[1,2048]{1,0:T(1,128)} %bitcast.4, f32[1,2048]{1,0:T(1,128)} %bitcast.5, s32[4,32]{1,0:T(4,128)} %bitcast.6, f32[4,32]{1,0:T(4,128)} %bitcast.7, bf16[1,2048,512]{2,1,0:T(8,128)(2,1)} %gate_hbm.1, bf16[1,2048,512]{2,1,0:T(8,128)(2,1)} %up_hbm.1, ...), custom_call_target="tpu_custom_call" | custom-call | tf_op jit(solution)/shard_map/moe/pallas_call | solution.py:253
  30.9 1.3 %copy.10 = bf16[32,256]{1,0:T(8,128)(2,1)} copy(bf16[32,256]{1,0:T(8,128)(2,1)} %moe.1) | data formatting | bytes 32768

commit v3 on v2

--- a/solution.py
+++ b/solution.py
@@ -9,7 +9,7 @@
 SIDE = 4
 CAP = 16
 BLK = 256
-CHUNKS = 1
+CHUNKS = 2
 OFFSETS = (
     ((2, 2), (1, 1), (3, 3), (1, 3), (3, 1), (0, 2), (2, 0), (0, 0)),
     ((1, 2), (2, 1), (3, 2), (2, 3), (0, 1), (0, 3), (1, 0), (3, 0)),
@@ -33,7 +33,7 @@
     out_ref,
     tok, gain, bias, routes, weights, w_in, w_out, swap_in, swap_out,
     out_buf, x_buf, y_buf, r_buf,
-    load_sem, wload_sem, swap_send, swap_recv, d_send, d_recv, r_send, r_recv, plane_sem,
+    load_sem, wload_sem, swap_send, swap_recv, d_send, d_recv, r_send, r_recv, near_sem, plane_sem,
 ):
     ep, tp = lax.axis_index("ep"), lax.axis_index("tp")
     z, x = ep // SIDE, ep % SIDE
@@ -43,6 +43,20 @@
 
     def chip(dz, dx):
         return ((z + dz) % SIDE) * SIDE + (x + dx) % SIDE
+
+    sibling = (ep, y * 2 + 1 - c)
+    barrier = pltpu.get_barrier_semaphore()
+
+    @pl.when(c == 1)
+    def _():
+        pl.semaphore_signal(barrier, inc=1, device_id=sibling, device_id_type=MESH)
+
+    for dz in range(SIDE):
+        for dx in range(SIDE):
+            if dz or dx:
+                pl.semaphore_signal(barrier, inc=1, device_id=(chip(dz, dx), y * 2 + 1), device_id_type=MESH)
+    for dy in range(1, SIDE):
+        pl.semaphore_signal(barrier, inc=1, device_id=(ep, ((y + dy) % SIDE) * 2 + 1), device_id_type=MESH)
 
     small = [
         pltpu.make_async_copy(src, dst, load_sem.at[i])
@@ -60,17 +74,26 @@
     for copy in big:
         copy.start()
 
-    barrier = pltpu.get_barrier_semaphore()
-    for dz in range(SIDE):
-        for dx in range(SIDE):
-            for dc in range(2):
-                if dz or dx or dc:
-                    pl.semaphore_signal(
-                        barrier, inc=1, device_id=(chip(dz, dx), y * 2 + (c + dc) % 2), device_id_type=MESH
-                    )
-    column = [(ep, ((y + dy) % SIDE) * 2 + c) for dy in range(1, SIDE)]
-    for there in column:
-        pl.semaphore_signal(barrier, inc=1, device_id=there, device_id_type=MESH)
+    @pl.when(c == 0)
+    def _():
+        pl.semaphore_wait(barrier, 1)
+        pl.semaphore_signal(near_sem, inc=1, device_id=sibling, device_id_type=MESH)
+
+    @pl.when(c == 1)
+    def _():
+        pl.semaphore_wait(near_sem, 1)
+
+    swaps = []
+    for i, (src, dst) in enumerate(
+        ((gate_hbm.at[0], swap_in.at[0]), (up_hbm.at[0], swap_in.at[1]), (down_hbm.at[0], swap_out))
+    ):
+        swaps.append(
+            pltpu.make_async_remote_copy(
+                src_ref=src, dst_ref=dst, send_sem=swap_send.at[i], recv_sem=swap_recv.at[i],
+                device_id=sibling, device_id_type=MESH,
+            )
+        )
+        swaps[-1].start()
 
     for copy in small:
         copy.wait()
@@ -102,17 +125,14 @@
     outgoing = jnp.dot(mine, normed, preferred_element_type=jnp.float32)
     out_buf[...] = outgoing.astype(jnp.bfloat16).reshape(out_buf.shape)
 
-    pl.semaphore_wait(barrier, 2 * SIDE * SIDE - 1 + SIDE - 1)
-
-    sibling = (ep, y * 2 + 1 - c)
-    swaps = []
-    for i, (src, dst) in enumerate(((w_in.at[0], swap_in.at[0]), (w_in.at[1], swap_in.at[1]), (w_out, swap_out))):
-        swaps.append(
-            pltpu.make_async_remote_copy(
-                src_ref=src, dst_ref=dst, send_sem=swap_send.at[i], recv_sem=swap_recv.at[i],
-                device_id=sibling, device_id_type=MESH,
-            )
-        )
+    @pl.when(c == 1)
+    def _():
+        pl.semaphore_wait(barrier, 2 * (SIDE * SIDE - 1 + SIDE - 1))
+        pl.semaphore_signal(near_sem, inc=1, device_id=sibling, device_id_type=MESH)
+
+    @pl.when(c == 0)
+    def _():
+        pl.semaphore_wait(near_sem, 1)
 
     def dispatch(i):
         dz, dx = offset(k, i)
@@ -132,12 +152,15 @@
     def _():
         x_buf[7] = out_buf[7]
 
-    for there in column:
-        pl.semaphore_signal(plane_sem, inc=1, device_id=there, device_id_type=MESH)
-
-    for load, swap in zip(big, swaps):
-        load.wait()
-        swap.start()
+    @pl.when(c == 1)
+    def _():
+        for dy in range(1, SIDE):
+            for core in range(2):
+                there = (ep, ((y + dy) % SIDE) * 2 + core)
+                pl.semaphore_signal(plane_sem, inc=1, device_id=there, device_id_type=MESH)
+
+    for copy in big:
+        copy.wait()
 
     def hidden_of(rows_in, both):
         gate = jnp.dot(rows_in, both[0], preferred_element_type=jnp.float32)
@@ -247,13 +270,13 @@
 def body(tokens, norm_gain, norm_bias, routes, route_weights, gate_w, up_w, down_w):
     rows, width = tokens.shape
     half = gate_w.shape[2]
-    hbm = pl.BlockSpec(memory_space=pl.ANY)
+    hbm = pl.BlockSpec(memory_space=pltpu.HBM)
     bf16, f32 = jnp.bfloat16, jnp.float32
     dma = pltpu.SemaphoreType.DMA
     return pl.pallas_call(
         kernel,
         name="moe",
-        out_shape=jax.ShapeDtypeStruct((rows, BLK), bf16),
+        out_shape=pltpu.VMEM((rows, BLK), bf16),
         in_specs=[hbm] * 8,
         out_specs=pl.BlockSpec(memory_space=pltpu.VMEM),
         scratch_shapes=[
@@ -272,10 +295,16 @@
             pltpu.VMEM((SIDE, 16, CAP, BLK), bf16),
             dma((5,)), dma((3,)), dma((3,)), dma((3,)), dma((8,)), dma((8,)), dma((4,)), dma((5,)),
             pltpu.SemaphoreType.REGULAR,
+            pltpu.SemaphoreType.REGULAR,
         ],
-        compiler_params=pltpu.CompilerParams(collective_id=0, has_side_effects=True),
+        compiler_params=pltpu.CompilerParams(collective_id=0, has_side_effects=True, vmem_limit_bytes=32 << 20),
     )(
-        tokens, norm_gain.reshape(1, width), norm_bias.reshape(1, width), routes.T, route_weights.T, gate_w, up_w, down_w
+        *(
+            pltpu.with_memory_space_constraint(a, pltpu.HBM)
+            for a in (
+                tokens, norm_gain.reshape(1, width), norm_bias.reshape(1, width), routes.T, route_weights.T, gate_w, up_w, down_w
+            )
+        )
     )
 
 

time: 32.4 us -> 30.2 us (0.932)
  Pallas kernels: 30.8 us -> 29.5 us
  local copies, waits for them, and re-layouts: 1.32 us -> 0.61 us
    pallas_call x1, Pallas kernels: 30.8 us -> 29.5 us  [body(): pl.pallas_call(kernel, name='moe', out_shape=pltpu.VMEM((rows, BLK), bf16...]
    unnamed x1, local copies, waits for them, and re-layouts: 1.32 us -> 0.61 us
where the time goes in v3:
time: 30.2 us; the launch traced here: 30.1 us
  Pallas kernels  29.5 us (98%)
  local copies, waits for them, and re-layouts  0.61 us (2%)
    pallas_call x1, Pallas kernels, body(): pl.pallas_call(kernel, name='moe', out_shape=pltpu.VMEM((rows, BLK), bf16...  29.5 us
    unnamed x1, local copies, waits for them, and re-layouts  0.61 us

profile of v3, /device:TPU:1, one launch (start us, length us, event | category | flops | bytes accessed | tf_op | source)
XLA Modules:
  0.0 30.1 jit_solution(1334868404189582891)
XLA Ops:
  0.0 29.5 %moe.1 = bf16[32,256]{1,0:T(8,128)(2,1)S(1)} custom-call(bf16[32,2048]{1,0:T(8,128)(2,1)} %tok_hbm.1, f32[1,2048]{1,0:T(1,128)} %bitcast.4, f32[1,2048]{1,0:T(1,128)} %bitcast.5, s32[4,32]{1,0:T(4,128)} %bitcast.6, f32[4,32]{1,0:T(4,128)} %bitcast.7, bf16[1,2048,512]{2,1,0:T(8,128)(2,1)} %gate_hbm.1, bf16[1,2048,512]{2,1,0:T(8,128)(2,1)} %up_hbm.1, ...), custom_call_target="tpu_custom_call" | custom-call | tf_op jit(solution)/shard_map/moe/pallas_call | solution.py:276
  29.5 0.6 %copy.10 = bf16[32,256]{1,0:T(8,128)(2,1)} copy(bf16[32,256]{1,0:T(8,128)(2,1)S(1)} %moe.1) | data formatting | bytes 32768

commit v4 on v3

--- a/solution.py
+++ b/solution.py
@@ -9,11 +9,19 @@
 SIDE = 4
 CAP = 16
 BLK = 256
-CHUNKS = 2
+CHUNKS = ((0, 1, 2, 7), (3, 4, 5, 6))
+ORDER = (0, 1, 2, 7, 3, 4, 5, 6)
 OFFSETS = (
     ((2, 2), (1, 1), (3, 3), (1, 3), (3, 1), (0, 2), (2, 0), (0, 0)),
-    ((1, 2), (2, 1), (3, 2), (2, 3), (0, 1), (0, 3), (1, 0), (3, 0)),
+    ((1, 2), (3, 2), (1, 0), (2, 1), (2, 3), (0, 1), (0, 3), (3, 0)),
 )
+
+
+GROUPS = ((1,), (3,), (2,), (0,))
+
+
+def sending(group, members):
+    return [(dy, i, h) for dy in group for i in members for h in range(2)]
 
 
 def offset(k, i):
@@ -141,12 +149,18 @@
             device_id=(chip(dz, dx), y * 2 + par), device_id_type=MESH,
         )
 
-    for i in range(7):
-        dispatch(i).start()
-
-    @pl.when(k == 1)
-    def _():
-        dispatch(7).start()
+    for i in ORDER:
+        if i == CHUNKS[1][0]:
+            for n in CHUNKS[0]:
+                if n < 7:
+                    dispatch(n).wait_send()
+        if i < 7:
+            dispatch(i).start()
+        else:
+
+            @pl.when(k == 1)
+            def _():
+                dispatch(7).start()
 
     @pl.when(k == 0)
     def _():
@@ -177,10 +191,8 @@
             device_id=(chip(SIDE - dz, SIDE - dx), ((y + dy) % SIDE) * 2 + h), device_id_type=MESH,
         )
 
-    per = 8 // CHUNKS
-    for chunk in range(CHUNKS):
-        first = chunk * per
-        for i in range(first, first + per):
+    for chunk, members in enumerate(CHUNKS):
+        for i in members:
             if i < 7:
                 dispatch(i).wait_recv()
             else:
@@ -189,7 +201,7 @@
                 def _():
                     dispatch(7).wait_recv()
 
-        rows_in = x_buf[first : first + per].reshape(per * CAP, x_buf.shape[2])
+        rows_in = jnp.concatenate([x_buf[i] for i in members], axis=0)
         hidden_own = hidden_of(rows_in, w_in)
         if chunk == 0:
             swaps[0].wait_recv()
@@ -198,26 +210,28 @@
         if chunk == 0:
             swaps[2].wait_recv()
             pl.semaphore_wait(plane_sem, SIDE - 1)
-        for dy in (2, 1, 3, 0):
-            for h in range(2):
-                cols = pl.ds(pl.multiple_of((((y + dy) % SIDE) * 2 + h) * BLK, BLK), BLK)
-                piece = jnp.dot(hidden_own, w_out[:, cols], preferred_element_type=jnp.float32)
-                piece += jnp.dot(hidden_swap, swap_out[:, cols], preferred_element_type=jnp.float32)
-                y_buf[first : first + per, dy, h] = piece.astype(jnp.bfloat16).reshape(per, CAP, BLK)
-            for i in range(first, first + per):
+        for group in GROUPS:
+            for dy in group:
                 for h in range(2):
-                    if i < 7 or dy:
-                        give_back(i, dy, h).start()
-                    else:
-                        local = (k == 0) & (c == h)
-
-                        @pl.when(local)
-                        def _():
-                            r_buf[0, 15] = y_buf[7, 0, h]
-
-                        @pl.when(jnp.logical_not(local))
-                        def _():
-                            give_back(7, 0, h).start()
+                    cols = pl.ds(pl.multiple_of((((y + dy) % SIDE) * 2 + h) * BLK, BLK), BLK)
+                    piece = jnp.dot(hidden_own, w_out[:, cols], preferred_element_type=jnp.float32)
+                    piece += jnp.dot(hidden_swap, swap_out[:, cols], preferred_element_type=jnp.float32)
+                    piece = piece.astype(jnp.bfloat16)
+                    for n, i in enumerate(members):
+                        y_buf[i, dy, h] = piece[n * CAP : (n + 1) * CAP]
+            for dy, i, h in sending(group, members):
+                if i < 7 or dy:
+                    give_back(i, dy, h).start()
+                else:
+                    local = (k == 0) & (c == h)
+
+                    @pl.when(local)
+                    def _():
+                        r_buf[0, 15] = y_buf[7, 0, h]
+
+                    @pl.when(jnp.logical_not(local))
+                    def _():
+                        give_back(7, 0, h).start()
 
     scaled = jnp.where(here, weight, 0.0).T
     high = scaled.astype(jnp.bfloat16)
@@ -245,7 +259,7 @@
 
     for swap in swaps:
         swap.wait_send()
-    for i in range(7):
+    for i in CHUNKS[1]:
         dispatch(i).wait_send()
 
     @pl.when(k == 1)

time: 30.2 us -> 28.3 us (0.937)
  Pallas kernels: 29.5 us -> 27.6 us
    pallas_call x1, Pallas kernels: 29.5 us -> 27.6 us  [body(): pl.pallas_call(kernel, name='moe', out_shape=pltpu.VMEM((rows, BLK), bf16...]
where the time goes in v4:
time: 28.3 us; the launch traced here: 28.2 us
  Pallas kernels  27.6 us (98%)
  local copies, waits for them, and re-layouts  0.61 us (2%)
    pallas_call x1, Pallas kernels, body(): pl.pallas_call(kernel, name='moe', out_shape=pltpu.VMEM((rows, BLK), bf16...  27.6 us
    unnamed x1, local copies, waits for them, and re-layouts  0.61 us

profile of v4, /device:TPU:1, one launch (start us, length us, event | category | flops | bytes accessed | tf_op | source)
XLA Modules:
  0.0 28.2 jit_solution(4705883859906898175)
XLA Ops:
  0.0 27.6 %moe.1 = bf16[32,256]{1,0:T(8,128)(2,1)S(1)} custom-call(bf16[32,2048]{1,0:T(8,128)(2,1)} %tok_hbm.1, f32[1,2048]{1,0:T(1,128)} %bitcast.4, f32[1,2048]{1,0:T(1,128)} %bitcast.5, s32[4,32]{1,0:T(4,128)} %bitcast.6, f32[4,32]{1,0:T(4,128)} %bitcast.7, bf16[1,2048,512]{2,1,0:T(8,128)(2,1)} %gate_hbm.1, bf16[1,2048,512]{2,1,0:T(8,128)(2,1)} %up_hbm.1, ...), custom_call_target="tpu_custom_call" | custom-call | tf_op jit(solution)/shard_map/moe/pallas_call | solution.py:290
  27.6 0.6 %copy.10 = bf16[32,256]{1,0:T(8,128)(2,1)} copy(bf16[32,256]{1,0:T(8,128)(2,1)S(1)} %moe.1) | data formatting | bytes 32768

commit v5 on v3

--- a/solution.py
+++ b/solution.py
@@ -9,11 +9,15 @@
 SIDE = 4
 CAP = 16
 BLK = 256
-CHUNKS = 2
+CHUNKS = ((0, 1, 2, 7), (3, 4, 5, 6))
+ORDER = (0, 1, 2, 7, 3, 4, 5, 6)
 OFFSETS = (
-    ((2, 2), (1, 1), (3, 3), (1, 3), (3, 1), (0, 2), (2, 0), (0, 0)),
-    ((1, 2), (2, 1), (3, 2), (2, 3), (0, 1), (0, 3), (1, 0), (3, 0)),
+    ((0, 3), (3, 0), (0, 2), (1, 3), (3, 1), (0, 1), (1, 0), (0, 0)),
+    ((2, 2), (1, 2), (2, 1), (3, 2), (2, 3), (2, 0), (1, 1), (3, 3)),
 )
+
+
+RETURNS = (1, 3, 2, 0)
 
 
 def offset(k, i):
@@ -38,8 +42,7 @@
     ep, tp = lax.axis_index("ep"), lax.axis_index("tp")
     z, x = ep // SIDE, ep % SIDE
     y, c = tp // 2, tp % 2
-    par = (z + x) % 2
-    k = (par + c) % 2
+    k = c
 
     def chip(dz, dx):
         return ((z + dz) % SIDE) * SIDE + (x + dx) % SIDE
@@ -51,10 +54,8 @@
     def _():
         pl.semaphore_signal(barrier, inc=1, device_id=sibling, device_id_type=MESH)
 
-    for dz in range(SIDE):
-        for dx in range(SIDE):
-            if dz or dx:
-                pl.semaphore_signal(barrier, inc=1, device_id=(chip(dz, dx), y * 2 + 1), device_id_type=MESH)
+    for dz, dx in sorted(OFFSETS[0][:7] + OFFSETS[1], key=lambda d: -min(d[0], 4 - d[0]) - min(d[1], 4 - d[1])):
+        pl.semaphore_signal(barrier, inc=1, device_id=(chip(dz, dx), y * 2 + 1), device_id_type=MESH)
     for dy in range(1, SIDE):
         pl.semaphore_signal(barrier, inc=1, device_id=(ep, ((y + dy) % SIDE) * 2 + 1), device_id_type=MESH)
 
@@ -83,17 +84,21 @@
     def _():
         pl.semaphore_wait(near_sem, 1)
 
-    swaps = []
-    for i, (src, dst) in enumerate(
-        ((gate_hbm.at[0], swap_in.at[0]), (up_hbm.at[0], swap_in.at[1]), (down_hbm.at[0], swap_out))
-    ):
-        swaps.append(
-            pltpu.make_async_remote_copy(
-                src_ref=src, dst_ref=dst, send_sem=swap_send.at[i], recv_sem=swap_recv.at[i],
-                device_id=sibling, device_id_type=MESH,
-            )
-        )
-        swaps[-1].start()
+    def columns(dy, width):
+        return pl.ds(pl.multiple_of(((y + dy) % SIDE) * width, width), width)
+
+    swaps = [(gate_hbm.at[0], swap_in.at[0]), (up_hbm.at[0], swap_in.at[1])]
+    for dy in RETURNS:
+        swaps.append((down_hbm.at[0, :, columns(dy, 2 * BLK)], swap_out.at[:, columns(dy, 2 * BLK)]))
+    swaps = [
+        pltpu.make_async_remote_copy(
+            src_ref=src, dst_ref=dst, send_sem=swap_send.at[i], recv_sem=swap_recv.at[i],
+            device_id=sibling, device_id_type=MESH,
+        )
+        for i, (src, dst) in enumerate(swaps)
+    ]
+    for swap in swaps:
+        swap.start()
 
     for copy in small:
         copy.wait()
@@ -138,15 +143,21 @@
         dz, dx = offset(k, i)
         return pltpu.make_async_remote_copy(
             src_ref=out_buf.at[i], dst_ref=x_buf.at[i], send_sem=d_send.at[i], recv_sem=d_recv.at[i],
-            device_id=(chip(dz, dx), y * 2 + par), device_id_type=MESH,
-        )
-
-    for i in range(7):
-        dispatch(i).start()
-
-    @pl.when(k == 1)
-    def _():
-        dispatch(7).start()
+            device_id=(chip(dz, dx), y * 2 + c), device_id_type=MESH,
+        )
+
+    for i in ORDER:
+        if i == CHUNKS[1][0]:
+            for n in CHUNKS[0]:
+                if n < 7:
+                    dispatch(n).wait_send()
+        if i < 7:
+            dispatch(i).start()
+        else:
+
+            @pl.when(k == 1)
+            def _():
+                dispatch(7).start()
 
     @pl.when(k == 0)
     def _():
@@ -177,10 +188,8 @@
             device_id=(chip(SIDE - dz, SIDE - dx), ((y + dy) % SIDE) * 2 + h), device_id_type=MESH,
         )
 
-    per = 8 // CHUNKS
-    for chunk in range(CHUNKS):
-        first = chunk * per
-        for i in range(first, first + per):
+    for chunk, members in enumerate(CHUNKS):
+        for i in members:
             if i < 7:
                 dispatch(i).wait_recv()
             else:
@@ -189,22 +198,25 @@
                 def _():
                     dispatch(7).wait_recv()
 
-        rows_in = x_buf[first : first + per].reshape(per * CAP, x_buf.shape[2])
+        rows_in = jnp.concatenate([x_buf[i] for i in members], axis=0)
         hidden_own = hidden_of(rows_in, w_in)
         if chunk == 0:
             swaps[0].wait_recv()
             swaps[1].wait_recv()
         hidden_swap = hidden_of(rows_in, swap_in)
         if chunk == 0:
-            swaps[2].wait_recv()
             pl.semaphore_wait(plane_sem, SIDE - 1)
-        for dy in (2, 1, 3, 0):
+        for step, dy in enumerate(RETURNS):
+            if chunk == 0:
+                swaps[2 + step].wait_recv()
             for h in range(2):
                 cols = pl.ds(pl.multiple_of((((y + dy) % SIDE) * 2 + h) * BLK, BLK), BLK)
                 piece = jnp.dot(hidden_own, w_out[:, cols], preferred_element_type=jnp.float32)
                 piece += jnp.dot(hidden_swap, swap_out[:, cols], preferred_element_type=jnp.float32)
-                y_buf[first : first + per, dy, h] = piece.astype(jnp.bfloat16).reshape(per, CAP, BLK)
-            for i in range(first, first + per):
+                piece = piece.astype(jnp.bfloat16)
+                for n, i in enumerate(members):
+                    y_buf[i, dy, h] = piece[n * CAP : (n + 1) * CAP]
+            for i in members:
                 for h in range(2):
                     if i < 7 or dy:
                         give_back(i, dy, h).start()
@@ -230,22 +242,23 @@
             device_id=sibling, device_id_type=MESH,
         )
 
-    arrived(r_buf.at[0, 0:15], 0).wait_recv()
-
-    @pl.when(k == 1)
-    def _():
-        arrived(r_buf.at[0, 15], 4).wait_recv()
-
-    for dy in (1, 3, 2):
-        arrived(r_buf.at[dy], dy).wait_recv()
     twice = jnp.zeros((2 * rows, BLK), jnp.float32)
-    for dy in range(SIDE):
+    for dy in (1, 3, 2, 0):
+        if dy:
+            arrived(r_buf.at[dy], dy).wait_recv()
+        else:
+            arrived(r_buf.at[0, 0:15], 0).wait_recv()
+
+            @pl.when(k == 1)
+            def _():
+                arrived(r_buf.at[0, 15], 4).wait_recv()
+
         twice += jnp.dot(both, r_buf[dy].reshape(slots, BLK), preferred_element_type=jnp.float32)
     out_ref[...] = (twice[:rows] + twice[rows:]).astype(out_ref.dtype)
 
     for swap in swaps:
         swap.wait_send()
-    for i in range(7):
+    for i in CHUNKS[1]:
         dispatch(i).wait_send()
 
     @pl.when(k == 1)
@@ -293,7 +306,7 @@
             pltpu.VMEM((8, CAP, width), bf16),
             pltpu.VMEM((8, SIDE, 2, CAP, BLK), bf16),
             pltpu.VMEM((SIDE, 16, CAP, BLK), bf16),
-            dma((5,)), dma((3,)), dma((3,)), dma((3,)), dma((8,)), dma((8,)), dma((4,)), dma((5,)),
+            dma((5,)), dma((3,)), dma((6,)), dma((6,)), dma((8,)), dma((8,)), dma((4,)), dma((5,)),
             pltpu.SemaphoreType.REGULAR,
             pltpu.SemaphoreType.REGULAR,
         ],

time: 30.2 us -> 27.6 us (0.914)
  Pallas kernels: 29.5 us -> 26.9 us
    pallas_call x1, Pallas kernels: 29.5 us -> 26.9 us  [body(): pl.pallas_call(kernel, name='moe', out_shape=pltpu.VMEM((rows, BLK), bf16...]
where the time goes in v5:
time: 27.6 us; the launch traced here: 27.5 us
  Pallas kernels  26.9 us (97%)
  local copies, waits for them, and re-layouts  0.61 us (2%)
    pallas_call x1, Pallas kernels, body(): pl.pallas_call(kernel, name='moe', out_shape=pltpu.VMEM((rows, BLK), bf16...  26.9 us
    unnamed x1, local copies, waits for them, and re-layouts  0.61 us

profile of v5, /device:TPU:1, one launch (start us, length us, event | category | flops | bytes accessed | tf_op | source)
XLA Modules:
  0.0 27.5 jit_solution(469748873878306364)
XLA Ops:
  0.0 26.9 %moe.1 = bf16[32,256]{1,0:T(8,128)(2,1)S(1)} custom-call(bf16[32,2048]{1,0:T(8,128)(2,1)} %tok_hbm.1, f32[1,2048]{1,0:T(1,128)} %bitcast.4, f32[1,2048]{1,0:T(1,128)} %bitcast.5, s32[4,32]{1,0:T(4,128)} %bitcast.6, f32[4,32]{1,0:T(4,128)} %bitcast.7, bf16[1,2048,512]{2,1,0:T(8,128)(2,1)} %gate_hbm.1, bf16[1,2048,512]{2,1,0:T(8,128)(2,1)} %up_hbm.1, ...), custom_call_target="tpu_custom_call" | custom-call | tf_op jit(solution)/shard_map/moe/pallas_call | solution.py:289
  26.9 0.6 %copy.10 = bf16[32,256]{1,0:T(8,128)(2,1)} copy(bf16[32,256]{1,0:T(8,128)(2,1)S(1)} %moe.1) | data formatting | bytes 32768

commit v6 on v5

--- a/solution.py
+++ b/solution.py
@@ -48,6 +48,15 @@
         return ((z + dz) % SIDE) * SIDE + (x + dx) % SIDE
 
     sibling = (ep, y * 2 + 1 - c)
+    small = [
+        pltpu.make_async_copy(src, dst, load_sem.at[i])
+        for i, (src, dst) in enumerate(
+            ((tok_hbm, tok), (gain_hbm, gain), (bias_hbm, bias), (routes_hbm, routes), (weights_hbm, weights))
+        )
+    ]
+    for copy in small:
+        copy.start()
+
     barrier = pltpu.get_barrier_semaphore()
 
     @pl.when(c == 1)
@@ -59,14 +68,6 @@
     for dy in range(1, SIDE):
         pl.semaphore_signal(barrier, inc=1, device_id=(ep, ((y + dy) % SIDE) * 2 + 1), device_id_type=MESH)
 
-    small = [
-        pltpu.make_async_copy(src, dst, load_sem.at[i])
-        for i, (src, dst) in enumerate(
-            ((tok_hbm, tok), (gain_hbm, gain), (bias_hbm, bias), (routes_hbm, routes), (weights_hbm, weights))
-        )
-    ]
-    for copy in small:
-        copy.start()
     big = [
         pltpu.make_async_copy(gate_hbm.at[0], w_in.at[0], wload_sem.at[0]),
         pltpu.make_async_copy(up_hbm.at[0], w_in.at[1], wload_sem.at[1]),

time: 27.6 us -> 27.6 us (level)
  no operation moved by 1% of the time
where the time goes in v6:
time: 27.6 us; the launch traced here: 27.5 us
  Pallas kernels  26.9 us (97%)
  local copies, waits for them, and re-layouts  0.61 us (2%)
    pallas_call x1, Pallas kernels, body(): pl.pallas_call(kernel, name='moe', out_shape=pltpu.VMEM((rows, BLK), bf16...  26.9 us
    unnamed x1, local copies, waits for them, and re-layouts  0.61 us

profile of v6, /device:TPU:1, one launch (start us, length us, event | category | flops | bytes accessed | tf_op | source)
XLA Modules:
  0.0 27.5 jit_solution(1952764333769581484)
XLA Ops:
  0.0 26.9 %moe.1 = bf16[32,256]{1,0:T(8,128)(2,1)S(1)} custom-call(bf16[32,2048]{1,0:T(8,128)(2,1)} %tok_hbm.1, f32[1,2048]{1,0:T(1,128)} %bitcast.4, f32[1,2048]{1,0:T(1,128)} %bitcast.5, s32[4,32]{1,0:T(4,128)} %bitcast.6, f32[4,32]{1,0:T(4,128)} %bitcast.7, bf16[1,2048,512]{2,1,0:T(8,128)(2,1)} %gate_hbm.1, bf16[1,2048,512]{2,1,0:T(8,128)(2,1)} %up_hbm.1, ...), custom_call_target="tpu_custom_call" | custom-call | tf_op jit(solution)/shard_map/moe/pallas_call | solution.py:290
  26.9 0.6 %copy.10 = bf16[32,256]{1,0:T(8,128)(2,1)} copy(bf16[32,256]{1,0:T(8,128)(2,1)S(1)} %moe.1) | data formatting | bytes 32768
